TPU v7x, 32 devices: a whole 2x2x4 slice. The times are simulated.
32 devices in a mesh: kv: 16 (over z, y, x), tp: 2 (over core).
Axes of the slice: x: 2, y: 2, z: 4, core: 2. Of those that a mesh axis runs over, the one named last changes fastest.
Arguments:
- tokens: bfloat16 [6144, 2048], P('kv', 'tp'), may hold values from -12 to 12
- query_weight: bfloat16 [2048, 2048], P(None, 'tp'), may hold values from -0.5 to 0.5
- key_weight: bfloat16 [2048, 1024], P(None, 'tp'), may hold values from -0.5 to 0.5
- value_weight: bfloat16 [2048, 1024], P(None, 'tp'), may hold values from -0.125 to 0.125
- out_weight: bfloat16 [2048, 2048], P(None, 'tp'), may hold values from -0.125 to 0.125
- chosen: int32 [96, 16], P('kv'), may hold values from 0 to 95, as said below
Outputs:
- mixed: bfloat16 [6144, 2048], P('kv', 'tp')
Inputs may be any that keep to these rules, and one draw needn't show every extreme that they name: `chosen`: row b names no block after b; its first entry is b and its next 3 entries are blocks of the same device as block b; entries may repeat. Over the rows of one device, the entries after the first 4 name at most 2 blocks, counting repeats, of any one other device, and some device names exactly 2 of another.
All inputs are finite; a program needn't handle non-finite values.
Results may differ from a plain program's by a relative error of at most 0.0072.
Values may be sent and summed in bfloat16 or wider, within the bound.
No kernel may reach another device: no remote copies, remote signals or barrier semaphores. Data moves between devices by JAX's collectives and lax.ppermute only.
A program may use at most 128 MiB of HBM per device.

v0:
```python
import jax
import jax.numpy as jnp
from jax import lax
from jax.sharding import PartitionSpec as P

HD = 128
BLK = 64
TOPB = 16
CAP = 2


def local(tokens, query_weight, key_weight, value_weight, out_weight, chosen):
    tok_rows = tokens.shape[0]
    query_cols = query_weight.shape[1]
    key_cols = key_weight.shape[1]
    key_heads = key_cols // HD
    query_heads = query_cols // HD
    group_size = query_heads // key_heads
    own_blocks = tok_rows // BLK
    device = lax.axis_index("kv")
    key_devices = lax.axis_size("kv")
    section = lax.all_gather(tokens, "tp", axis=1, tiled=True)
    query_sum = jnp.dot(section, query_weight, preferred_element_type=jnp.float32)
    key_sum = jnp.dot(section, key_weight, preferred_element_type=jnp.float32)
    value_sum = jnp.dot(section, value_weight, preferred_element_type=jnp.float32)
    queries = query_sum.astype(jnp.bfloat16)
    paired = jnp.concatenate([key_sum.astype(jnp.bfloat16), value_sum.astype(jnp.bfloat16)], axis=1)
    own_pairs = paired.reshape(own_blocks, BLK, 2 * key_cols)
    wanted = chosen.reshape(-1)
    holder = wanted // own_blocks
    within = wanted % own_blocks
    remote = holder != device
    slot_index = jnp.arange(wanted.shape[0])
    earlier = (
        (slot_index[None, :] < slot_index[:, None])
        & (holder[None, :] == holder[:, None])
        & remote[None, :]
    )
    places = jnp.sum(earlier.astype(jnp.int32), axis=1)
    owner_ids = jnp.arange(key_devices)[:, None, None]
    place_ids = jnp.arange(CAP)[None, :, None]
    matches = (
        remote[None, None, :]
        & (holder[None, None, :] == owner_ids)
        & (places[None, None, :] == place_ids)
    )
    request_table = jnp.sum(jnp.where(matches, within[None, None, :], 0), axis=2)
    incoming = lax.all_to_all(request_table, "kv", split_axis=0, concat_axis=0, tiled=True)
    outgoing = jnp.take(own_pairs, incoming.reshape(-1), axis=0).reshape(
        key_devices, CAP, BLK, 2 * key_cols
    )
    arrived = lax.all_to_all(outgoing, "kv", split_axis=0, concat_axis=0, tiled=True)
    slot_ids = holder * CAP + jnp.minimum(places, CAP - 1)
    from_far = jnp.take(arrived.reshape(key_devices * CAP, BLK, 2 * key_cols), slot_ids, axis=0)
    from_near = jnp.take(own_pairs, within, axis=0)
    fetched = jnp.where(remote[:, None, None], from_far, from_near)
    fetched = fetched.reshape(own_blocks, TOPB * BLK, 2 * key_cols)
    got_keys = fetched[:, :, :key_cols].reshape(own_blocks, TOPB * BLK, key_heads, HD)
    got_values = fetched[:, :, key_cols:].reshape(own_blocks, TOPB * BLK, key_heads, HD)
    grouped = queries.reshape(own_blocks, BLK, key_heads, group_size, HD)
    scores = jnp.einsum(
        "bqkgd,bskd->bkgqs", grouped, got_keys, preferred_element_type=jnp.float32
    ) * HD ** (-0.5)
    slot_order = jnp.arange(TOPB)
    repeats = jnp.any(
        (chosen[:, :, None] == chosen[:, None, :])
        & (slot_order[None, None, :] < slot_order[None, :, None]),
        axis=2,
    )
    first_block = device * own_blocks
    query_pos = (first_block + jnp.arange(own_blocks))[:, None] * BLK + jnp.arange(BLK)[None, :]
    key_pos = (chosen[:, :, None] * BLK + jnp.arange(BLK)[None, None, :]).reshape(
        own_blocks, TOPB * BLK
    )
    fresh_slot = jnp.broadcast_to((~repeats)[:, :, None], (own_blocks, TOPB, BLK)).reshape(
        own_blocks, TOPB * BLK
    )
    visible = fresh_slot[:, None, :] & (key_pos[:, None, :] <= query_pos[:, :, None])
    scores = jnp.where(visible[:, None, None], scores, -jnp.inf)
    row_peak = jnp.max(scores, axis=-1, keepdims=True)
    weights = jnp.exp(scores - row_peak)
    row_total = jnp.sum(weights, axis=-1)
    mixed_heads = jnp.einsum(
        "bkgqs,bskd->bqkgd",
        weights.astype(jnp.bfloat16),
        got_values,
        preferred_element_type=jnp.float32,
    )
    mixed_heads = mixed_heads / jnp.transpose(row_total, (0, 3, 1, 2))[..., None]
    heads_out = mixed_heads.astype(jnp.bfloat16).reshape(tok_rows, query_cols)
    result = jnp.dot(
        lax.all_gather(heads_out, "tp", axis=1, tiled=True),
        out_weight,
        preferred_element_type=jnp.float32,
    )
    return result.astype(jnp.bfloat16)


def solution(mesh):
    return jax.shard_map(
        local,
        mesh=mesh,
        in_specs=(
            P("kv", "tp"),
            P(None, "tp"),
            P(None, "tp"),
            P(None, "tp"),
            P(None, "tp"),
            P("kv", None),
        ),
        out_specs=P("kv", "tp"),
        check_vma=False,
    )
```

profile of v0, /device:TPU:0, one launch (start us, length us, event | category | flops | bytes accessed | tf_op | source)
XLA Modules:
  0.0 226.4 jit_solution(6971338226301510048)
XLA Ops:
  6.5 0.7 all-gather.3.cloned.1.call-update
  7.3 0.7 broadcast_multiply_fusion
  8.0 0.7 fusion.18
  9.4 15.4 %all_to_all.14 = s32[16,1,2]{2,1,0:T(1,128)S(1)} all-to-all(s32[16,1,2]{2,1,0:T(1,128)S(1)} %copy.33), channel_id=1, replica_groups=mesh['kv'=16,'tp'=2] {'kv'}, dimensions={0} | all-to-all | bytes 256 | tf_op jit(solution)/shard_map/all_to_all | solution.py:48
  26.3 2.4 %convolution_convert_fusion.2 = bf16[384,512]{1,0:T(8,128)(2,1)S(1)} fusion(bf16[384,2048]{1,0:T(8,128)(2,1)} %all-gather.3.cloned.1.call-done, bf16[2048,512]{1,0:T(8,128)(2,1)S(1)} %copy-done), kind=kOutput, calls=%fused_computation.22 | convolution fusion | flops 805502976 | bytes 4063232 | tf_op jit(solution)/shard_map/dot_general | solution.py:25
  28.7 3.0 %convolution_convert_fusion.3 = bf16[384,512]{1,0:T(8,128)(2,1)S(1)} fusion(bf16[384,2048]{1,0:T(8,128)(2,1)} %all-gather.3.cloned.1.call-done, bf16[2048,512]{1,0:T(8,128)(2,1)} %param.8), kind=kOutput, calls=%fused_computation.23 | convolution fusion | flops 805502976 | bytes 4063232 | tf_op jit(solution)/shard_map/dot_general | solution.py:24
  31.8 2.8 %gather_fusion = bf16[32,64,1024]{2,1,0:T(8,128)(2,1)} fusion(bf16[6,64,1024]{2,1,0:T(8,128)(2,1)S(1)} %bitcast.62, s32[1024]{0:T(1024)S(1)} %pad_clamp_fusion.2), kind=kCustom, calls=%fused_computation | custom fusion | bytes 8388736 | tf_op jit(solution)/shard_map/jit(_take)/gather | solution.py:49
  34.6 4.6 %broadcast_select_fusion = bf16[16,2,64,1024]{3,2,1,0:T(8,128)(2,1)} fusion(bf16[16,2,64,1024]{3,2,1,0:T(8,128)(2,1)} %bitcast.67, pred[16,2]{1,0:T(8,128)(4,1)S(1)} %copy.35), kind=kLoop, calls=%fused_computation.16 | loop fusion | flops 2097152 | bytes 8388640 | tf_op jit(solution)/shard_map/jit(_take)/select_n | solution.py:49
  39.2 4.7 %all-to-all-start.1 = ((bf16[16,2,64,1024]{3,2,1,0:T(8,128)(2,1)}), bf16[16,2,64,1024]{3,2,1,0:T(8,128)(2,1)}, u32[]{:S(2)}, u32[]{:S(2)}) async-start(bf16[16,2,64,1024]{3,2,1,0:T(8,128)(2,1)} %broadcast_select_fusion), calls=%async_computation.1 | async-start | bytes 8388608 | tf_op jit(solution)/shard_map/all_to_all | solution.py:52
  46.1 4.5 %convolution_convert_fusion.1 = bf16[384,1024]{1,0:T(8,128)(2,1)S(1)} fusion(bf16[384,2048]{1,0:T(8,128)(2,1)} %all-gather.3.cloned.1.call-done, bf16[2048,1024]{1,0:T(8,128)(2,1)} %param.7), kind=kOutput, calls=%fused_computation.21 | convolution fusion | flops 1611005952 | bytes 6553600 | tf_op jit(solution)/shard_map/dot_general | solution.py:23
  51.1 7.1 %gather_fusion.2 = bf16[96,64,1024]{2,1,0:T(8,128)(2,1)} fusion(bf16[6,64,1024]{2,1,0:T(8,128)(2,1)S(1)} %bitcast.63, s32[1024]{0:T(1024)S(1)} %get-tuple-element.20), kind=kCustom, calls=%fused_computation.2 | custom fusion | bytes 25166208 | tf_op jit(solution)/shard_map/jit(_take)/gather | solution.py:55
  58.1 64.2 %all-to-all-done.1 = bf16[16,2,64,1024]{3,2,1,0:T(8,128)(2,1)} async-done(((bf16[16,2,64,1024]{3,2,1,0:T(8,128)(2,1)}), bf16[16,2,64,1024]{3,2,1,0:T(8,128)(2,1)}, u32[]{:S(2)}, u32[]{:S(2)}) %all-to-all-start.1) | async-done | bytes 4194336 | tf_op jit(solution)/shard_map/all_to_all | solution.py:52
  122.4 8.7 %gather_fusion.1 = bf16[96,64,1024]{2,1,0:T(8,128)(2,1)} fusion(bf16[32,64,1024]{2,1,0:T(8,128)(2,1)} %bitcast.5, s32[1024]{0:T(1024)S(1)} %get-tuple-element.21), kind=kCustom, calls=%fused_computation.1 | custom fusion | bytes 25166208 | tf_op jit(solution)/shard_map/jit(_take)/gather | solution.py:54
  131.0 9.0 %fusion = bf16[6,1024,1024]{2,1,0:T(8,128)(2,1)S(1)} fusion(pred[6,1024]{1,0:T(8,128)(4,1)S(1)} %broadcast_in_dim.114, pred[6,1024]{1,0:T(8,128)(4,1)S(1)} %broadcast_in_dim.106, pred[6,1024]{1,0:T(8,128)(4,1)S(1)} %broadcast_in_dim.103, bf16[6,1024,1024]{2,1,0:T(8,128)(2,1)} %bitcast.64, bf16[6,1024,1024]{2,1,0:T(8,128)(2,1)} %bitcast.65), kind=kLoop, calls=%fused_computation.5 | loop fusion | flops 18874368 | bytes 37767168 | tf_op jit(solution)/shard_map/jit(_where)/select_n | solution.py:56
  140.0 5.2 %fusion.24 = (bf16[6,1024,512]{2,1,0:T(8,128)(2,1)}, bf16[6,1024,512]{2,1,0:T(8,128)(2,1)}) fusion(bf16[6,1024,1024]{2,1,0:T(8,128)(2,1)S(1)} %fusion), kind=kLoop, calls=%fused_computation.72 | loop fusion | bytes 25165824 | tf_op jit(solution)/shard_map/slice | solution.py:58
  145.1 8.6 %copy.37 = bf16[6,1024,512]{1,2,0:T(8,128)(2,1)} copy(bf16[6,1024,512]{2,1,0:T(8,128)(2,1)} %get-tuple-element.9) | data formatting | bytes 12582912 | tf_op jit(solution)/shard_map/slice | solution.py:58
  153.8 8.7 %copy.36 = bf16[6,1024,512]{1,2,0:T(8,128)(2,1)} copy(bf16[6,1024,512]{2,1,0:T(8,128)(2,1)} %get-tuple-element.10) | data formatting | bytes 12582912 | tf_op jit(solution)/shard_map/slice | solution.py:59
  162.4 9.8 %fusion.3 = (f32[6,4,2,64]{3,2,1,0:T(2,128)S(1)}, f32[6,4,1024,64,2]{2,3,4,1,0:T(8,128)}) fusion(pred[6,64,1024]{2,1,0:T(8,128)(4,1)S(1)} %compare_and_fusion, bf16[6,1024,4,128,1]{1,3,4,2,0:T(8,128)(2,1)} %bitcast.66, bf16[6,64,4,2,128]{4,3,2,1,0:T(2,128)(2,1)S(1)} %reshape.419), kind=kOutput, calls=%fused_computation.10 | convolution fusion | flops 814740480 | bytes 20066304 | tf_op jit(solution)/shard_map/bqkgd,bskd->bkgqs/dot_general | solution.py:61
  172.2 6.6 %fusion.1 = f32[6,4,2,64]{3,2,1,0:T(2,128)S(1)} fusion(f32[6,4,1024,64,2]{2,3,4,1,0:T(8,128)} %get-tuple-element.19, f32[6,4,2,64]{3,2,1,0:T(2,128)S(1)} %get-tuple-element.18, pred[6,64,1024]{2,1,0:T(8,128)(4,1)S(1)} %compare_and_fusion), kind=kLoop, calls=%fused_computation.8 | loop fusion | flops 12579840 | bytes 13000704 | tf_op jit(solution)/shard_map/reduce_sum | solution.py:82
  178.8 9.9 %fusion.10 = bf16[6,64,4,2,128]{4,1,3,2,0:T(8,128)(2,1)S(1)} fusion(bf16[6,1024,4,128,1]{1,3,4,2,0:T(8,128)(2,1)} %bitcast.68, f32[6,4,1024,64,2]{2,3,4,1,0:T(8,128)} %get-tuple-element.19, f32[6,4,2,64]{3,2,1,0:T(2,128)S(1)} %get-tuple-element.18, pred[6,64,1024]{2,1,0:T(8,128)(4,1)S(1)} %compare_and_fusion, f32[6,64,4,2]{1,3,2,0:T(2,128)S(1)} %bitcast.69), kind=kOutput, calls=%fused_computation.18 | convolution fusion | flops 818675712 | bytes 20078592 | tf_op jit(solution)/shard_map/bkgqs,bskd->bqkgd/dot_general | solution.py:83
  188.7 0.8 copy.41
  189.5 1.4 reshape.420
  191.0 23.2 %all-gather.5.cloned.1.call-done = bf16[384,2048]{1,0:T(8,128)(2,1)} async-done(((bf16[384,1024]{1,0:T(8,128)(2,1)}), bf16[384,2048]{1,0:T(8,128)(2,1)}) %all-gather.5.cloned.1.call-update) | async-done | bytes 1572880 | tf_op jit(solution)/shard_map/all_gather | solution.py:92
  214.2 5.3 %convolution_convert_fusion = bf16[384,1024]{1,0:T(8,128)(2,1)} fusion(bf16[384,2048]{1,0:T(8,128)(2,1)} %all-gather.5.cloned.1.call-done, bf16[2048,1024]{1,0:T(8,128)(2,1)} %param.10), kind=kOutput, calls=%fused_computation.20 | convolution fusion | flops 1611005952 | bytes 6553600 | tf_op jit(solution)/shard_map/dot_general | solution.py:91
  (57 shorter events, 4.9 us)
Async XLA Ops:
  6.5 19.8 %copy-start = (bf16[2048,512]{1,0:T(8,128)(2,1)S(1)}, bf16[2048,512]{1,0:T(8,128)(2,1)}, u32[]{:S(2)}) copy-start(bf16[2048,512]{1,0:T(8,128)(2,1)} %param.9) | copy-start | bytes 6291460
  6.5 19.8 %all-gather.3.cloned.1.call-start = ((), (), s32[]{:S(2)}) async-start(), calls=%async_computation.2 | async-start | bytes 2359296 | tf_op jit(solution)/shard_map/all_gather | solution.py:22
  39.2 5.0 %copy-start.2 = (s32[6,16]{1,0:T(8,128)S(1)}, s32[6,16]{1,0:T(8,128)}, u32[]{:S(2)}) copy-start(s32[6,16]{1,0:T(8,128)} %param.11) | copy-start | bytes 1156
  39.2 83.2 %all-to-all-start.1 = ((bf16[16,2,64,1024]{3,2,1,0:T(8,128)(2,1)}), bf16[16,2,64,1024]{3,2,1,0:T(8,128)(2,1)}, u32[]{:S(2)}, u32[]{:S(2)}) async-start(bf16[16,2,64,1024]{3,2,1,0:T(8,128)(2,1)} %broadcast_select_fusion), calls=%async_computation.1 | async-start | bytes 8388608 | tf_op jit(solution)/shard_map/all_to_all | solution.py:52
  43.9 170.3 %all-gather.5.cloned.1.call-start = ((), (), s32[]{:S(2)}) async-start(), calls=%async_computation.3 | async-start | bytes 2359296 | tf_op jit(solution)/shard_map/all_gather | solution.py:92
  189.5 30.1 %copy-start.1 = (bf16[2048,512]{1,0:T(8,128)(2,1)S(1)}, bf16[2048,512]{1,0:T(8,128)(2,1)}, u32[]{:S(2)}) copy-start(bf16[2048,512]{1,0:T(8,128)(2,1)} %param.9) | copy-start | bytes 6291460
Sparse Core Ops, SparseCore 0:
  8.9 12.5 all-gather.2
  191.1 23.0 all-gather.4
where the time goes:
time: 227 us; the launch traced here: 226 us
  waiting for transfers between devices  88.2 us (39%)
  local copies, waits for them, and re-layouts  46.1 us (20%)
  matrix products  34.9 us (15%)
  other arithmetic  23.4 us (10%)
  blocking collectives  15.4 us (7%)
  between operations  13.7 us (6%)
  starting transfers between devices  4.74 us (2%)
    all_to_all x1, waiting for transfers between devices, local(): lax.all_to_all(outgoing, 'kv', split_axis=0, concat_axis=0, tiled=True)  64.2 us
    all_gather x1, waiting for transfers between devices, local(): lax.all_gather(heads_out, 'tp', axis=1, tiled=True)  23.2 us
    all_to_all x1, blocking collectives, local(): lax.all_to_all(request_table, 'kv', split_axis=0, concat_axis=0, tiled=True)  15.4 us
    slice x2, local copies, waits for them, and re-layouts, local(): fetched[:, :, :key_cols].reshape(own_blocks, TOPB * BLK, key_heads, HD)  13.8 us
    dot_general x1, matrix products, local(): jnp.einsum('bkgqs,bskd->bqkgd', weights.astype(jnp.bfloat16), got_values,...  9.89 us
    dot_general x1, matrix products, local(): jnp.einsum('bqkgd,bskd->bkgqs', grouped, got_keys, preferred_element_type...  9.77 us
    select_n x1, other arithmetic, local(): fetched = jnp.where(remote[:, None, None], from_far, from_near)  8.96 us
    slice x1, local copies, waits for them, and re-layouts, local(): fetched[:, :, key_cols:].reshape(own_blocks, TOPB * BLK, key_heads, HD)  8.67 us
  transfers between devices with their start and end apart: 3, of which 2 were waited for; matrix products, arithmetic and copies ran while one was open for 8% of the time, Pallas kernels for 0%

commit v1 on v0

--- a/solution.py
+++ b/solution.py
@@ -7,6 +7,17 @@
 BLK = 64
 TOPB = 16
 CAP = 2
+
+
+def in_blocks(x, dim, devices):
+    before, after = (x.shape[:dim], x.shape[dim + 1 :])
+    return jnp.moveaxis(x.reshape(*before, devices, -1, *after), dim, 0)
+
+
+def laid_out(blocks, dim):
+    blocks = jnp.moveaxis(blocks, 0, dim)
+    dims = blocks.shape
+    return blocks.reshape(*dims[:dim], dims[dim] * dims[dim + 1], *dims[dim + 2 :])
 
 
 def local(tokens, query_weight, key_weight, value_weight, out_weight, chosen):
@@ -45,7 +56,14 @@
         & (places[None, None, :] == place_ids)
     )
     request_table = jnp.sum(jnp.where(matches, within[None, None, :], 0), axis=2)
-    incoming = lax.all_to_all(request_table, "kv", split_axis=0, concat_axis=0, tiled=True)
+    devices, index = (lax.axis_size("kv"), lax.axis_index("kv"))
+    pieces = in_blocks(request_table, 0, devices)
+    done = [pieces[index]]
+    for step in range(1, devices):
+        sent = pieces[(index + step) % devices]
+        done.append(lax.ppermute(sent, "kv", [(i, (i + step) % devices) for i in range(devices)]))
+    pieces = jnp.stack(done)[(index - jnp.arange(devices)) % devices]
+    incoming = laid_out(pieces, 0)
     outgoing = jnp.take(own_pairs, incoming.reshape(-1), axis=0).reshape(
         key_devices, CAP, BLK, 2 * key_cols
     )

time: 227 us -> 243 us (1.070)
  starting transfers between devices: 4.74 us -> 32.4 us
  blocking collectives: 15.4 us -> 0 us
  waiting for transfers between devices: 88.2 us -> 92.5 us
    ppermute x0 -> x15, starting transfers between devices: none -> 27.6 us  [local(): lax.ppermute(sent, 'kv', [(i, (i + step) % devices) for i in range(device...]
    all_to_all x1 -> x0, blocking collectives: 15.4 us -> none  [local(): lax.all_to_all(request_table, 'kv', split_axis=0, concat_axis=0, tiled=True)]
    ppermute x0 -> x15, waiting for transfers between devices: none -> 7.18 us  [local(): lax.ppermute(sent, 'kv', [(i, (i + step) % devices) for i in range(device...]
    all_to_all x1, waiting for transfers between devices: 64.2 us -> 61.2 us  [local(): lax.all_to_all(outgoing, 'kv', split_axis=0, concat_axis=0, tiled=True)]
  transfers between devices with their start and end apart: 3 -> 18, of which waited for: 2 -> 5; matrix products, arithmetic and copies ran while one was open for 8% -> 7% of each run, Pallas kernels for 0% -> 0%
where the time goes in v1:
time: 243 us
  waiting for transfers between devices  92.5 us (38%)
  local copies, waits for them, and re-layouts  46.2 us (19%)
  matrix products  34.9 us (14%)
  starting transfers between devices  32.4 us (13%)
  other arithmetic  22.7 us (9%)
  between operations  13.9 us (6%)
    all_to_all x1, waiting for transfers between devices, local(): lax.all_to_all(outgoing, 'kv', split_axis=0, concat_axis=0, tiled=True)  61.2 us
    ppermute x15, starting transfers between devices, local(): lax.ppermute(sent, 'kv', [(i, (i + step) % devices) for i in range(device...  27.6 us
    all_gather x1, waiting for transfers between devices, local(): lax.all_gather(heads_out, 'tp', axis=1, tiled=True)  23.4 us
    slice x2, local copies, waits for them, and re-layouts, local(): fetched[:, :, :key_cols].reshape(own_blocks, TOPB * BLK, key_heads, HD)  13.8 us
    dot_general x1, matrix products, local(): jnp.einsum('bkgqs,bskd->bqkgd', weights.astype(jnp.bfloat16), got_values,...  9.89 us
    dot_general x1, matrix products, local(): jnp.einsum('bqkgd,bskd->bkgqs', grouped, got_keys, preferred_element_type...  9.75 us
    select_n x1, other arithmetic, local(): fetched = jnp.where(remote[:, None, None], from_far, from_near)  8.96 us
    slice x1, local copies, waits for them, and re-layouts, local(): fetched[:, :, key_cols:].reshape(own_blocks, TOPB * BLK, key_heads, HD)  8.7 us
  transfers between devices with their start and end apart: 18, of which 5 were waited for; matrix products, arithmetic and copies ran while one was open for 7% of the time, Pallas kernels for 0%

profile of v1, /device:TPU:0, one launch (start us, length us, event | category | flops | bytes accessed | tf_op | source)
XLA Modules:
  0.0 242.6 jit_solution(15196090712416741852)
XLA Ops:
  9.6 7.0 %collective-permute-start.14 = (s32[1,2]{0,1:T(2,128)S(1)}, s32[1,2]{0,1:T(2,128)S(1)}, u32[]{:S(2)}, u32[]{:S(2)}) collective-permute-start(s32[1,2]{0,1:T(2,128)S(1)} %get-tuple-element.16), channel_id=1, source_target_pairs={{0,30},{2,0},{4,2},{6,4},{8,6},{10,8},{12,10},{14,12},{16,14},{18,... | collective-permute-start | bytes 32 | tf_op jit(solution)/shard_map/ppermute | solution.py:64
  19.4 4.5 %collective-permute-start.9 = (s32[1,2]{0,1:T(2,128)S(1)}, s32[1,2]{0,1:T(2,128)S(1)}, u32[]{:S(2)}, u32[]{:S(2)}) collective-permute-start(s32[1,2]{0,1:T(2,128)S(1)} %get-tuple-element.21), channel_id=1, source_target_pairs={{0,20},{2,22},{4,24},{6,26},{8,28},{10,30},{12,0},{14,2},{16,4},{1... | collective-permute-start | bytes 32 | tf_op jit(solution)/shard_map/ppermute | solution.py:64
  25.5 2.6 %collective-permute-start.6 = (s32[1,2]{0,1:T(2,128)S(1)}, s32[1,2]{0,1:T(2,128)S(1)}, u32[]{:S(2)}, u32[]{:S(2)}) collective-permute-start(s32[1,2]{0,1:T(2,128)S(1)} %get-tuple-element.24), channel_id=1, source_target_pairs={{0,14},{2,16},{4,18},{6,20},{8,22},{10,24},{12,26},{14,28},{16,30}... | collective-permute-start | bytes 32 | tf_op jit(solution)/shard_map/ppermute | solution.py:64
  28.1 2.5 %collective-permute-start.5 = (s32[1,2]{0,1:T(2,128)S(1)}, s32[1,2]{0,1:T(2,128)S(1)}, u32[]{:S(2)}, u32[]{:S(2)}) collective-permute-start(s32[1,2]{0,1:T(2,128)S(1)} %get-tuple-element.25), channel_id=1, source_target_pairs={{0,12},{2,14},{4,16},{6,18},{8,20},{10,22},{12,24},{14,26},{16,28}... | collective-permute-start | bytes 32 | tf_op jit(solution)/shard_map/ppermute | solution.py:64
  33.2 3.3 %collective-permute-start.2 = (s32[1,2]{0,1:T(2,128)S(1)}, s32[1,2]{0,1:T(2,128)S(1)}, u32[]{:S(2)}, u32[]{:S(2)}) collective-permute-start(s32[1,2]{0,1:T(2,128)S(1)} %get-tuple-element.28), channel_id=1, source_target_pairs={{0,6},{2,8},{4,10},{6,12},{8,14},{10,16},{12,18},{14,20},{16,22},{... | collective-permute-start | bytes 32 | tf_op jit(solution)/shard_map/ppermute | solution.py:64
  37.3 3.0 %collective-permute-done.2 = s32[1,2]{0,1:T(2,128)S(1)} collective-permute-done((s32[1,2]{0,1:T(2,128)S(1)}, s32[1,2]{0,1:T(2,128)S(1)}, u32[]{:S(2)}, u32[]{:S(2)}) %collective-permute-start.2) | collective-permute-done | bytes 40 | tf_op jit(solution)/shard_map/ppermute | solution.py:64
  45.4 2.4 convolution_convert_fusion.2
  47.8 3.0 %convolution_convert_fusion.3 = bf16[384,512]{1,0:T(8,128)(2,1)S(1)} fusion(bf16[384,2048]{1,0:T(8,128)(2,1)} %all-gather.3.cloned.1.call-done, bf16[2048,512]{1,0:T(8,128)(2,1)} %param.8), kind=kOutput, calls=%fused_computation.24 | convolution fusion | flops 805502976 | bytes 4063232 | tf_op jit(solution)/shard_map/dot_general | solution.py:35
  51.0 2.8 %gather_fusion.1 = bf16[32,64,1024]{2,1,0:T(8,128)(2,1)} fusion(bf16[6,64,1024]{2,1,0:T(8,128)(2,1)S(1)} %bitcast.79, s32[1024]{0:T(1024)S(1)} %pad_clamp_fusion.2), kind=kCustom, calls=%fused_computation.1 | custom fusion | bytes 8388736 | tf_op jit(solution)/shard_map/jit(_take)/gather | solution.py:67
  53.7 4.6 %broadcast_select_fusion = bf16[16,2,64,1024]{3,2,1,0:T(8,128)(2,1)} fusion(bf16[16,2,64,1024]{3,2,1,0:T(8,128)(2,1)} %bitcast.84, pred[16,2]{1,0:T(8,128)(4,1)S(1)} %compare_and_fusion.1), kind=kLoop, calls=%fused_computation.17 | loop fusion | flops 2097152 | bytes 8388640 | tf_op jit(solution)/shard_map/jit(_take)/select_n | solution.py:67
  58.3 4.7 %all-to-all-start = ((bf16[16,2,64,1024]{3,2,1,0:T(8,128)(2,1)}), bf16[16,2,64,1024]{3,2,1,0:T(8,128)(2,1)}, u32[]{:S(2)}, u32[]{:S(2)}) async-start(bf16[16,2,64,1024]{3,2,1,0:T(8,128)(2,1)} %broadcast_select_fusion), calls=%async_computation | async-start | bytes 8388608 | tf_op jit(solution)/shard_map/all_to_all | solution.py:70
  65.2 4.5 %convolution_convert_fusion.1 = bf16[384,1024]{1,0:T(8,128)(2,1)S(1)} fusion(bf16[384,2048]{1,0:T(8,128)(2,1)} %all-gather.3.cloned.1.call-done, bf16[2048,1024]{1,0:T(8,128)(2,1)} %param.7), kind=kOutput, calls=%fused_computation.22 | convolution fusion | flops 1611005952 | bytes 6553600 | tf_op jit(solution)/shard_map/dot_general | solution.py:34
  70.2 7.0 %gather_fusion.3 = bf16[96,64,1024]{2,1,0:T(8,128)(2,1)} fusion(bf16[6,64,1024]{2,1,0:T(8,128)(2,1)S(1)} %bitcast.80, s32[1024]{0:T(1024)S(1)} %get-tuple-element.36), kind=kCustom, calls=%fused_computation.3 | custom fusion | bytes 25166208 | tf_op jit(solution)/shard_map/jit(_take)/gather | solution.py:73
  77.2 61.2 %all-to-all-done = bf16[16,2,64,1024]{3,2,1,0:T(8,128)(2,1)} async-done(((bf16[16,2,64,1024]{3,2,1,0:T(8,128)(2,1)}), bf16[16,2,64,1024]{3,2,1,0:T(8,128)(2,1)}, u32[]{:S(2)}, u32[]{:S(2)}) %all-to-all-start) | async-done | bytes 4194336 | tf_op jit(solution)/shard_map/all_to_all | solution.py:70
  138.4 8.7 %gather_fusion.2 = bf16[96,64,1024]{2,1,0:T(8,128)(2,1)} fusion(bf16[32,64,1024]{2,1,0:T(8,128)(2,1)} %bitcast.21, s32[1024]{0:T(1024)S(1)} %get-tuple-element.37), kind=kCustom, calls=%fused_computation.2 | custom fusion | bytes 25166208 | tf_op jit(solution)/shard_map/jit(_take)/gather | solution.py:72
  147.1 9.0 %fusion = bf16[6,1024,1024]{2,1,0:T(8,128)(2,1)S(1)} fusion(pred[6,1024]{1,0:T(8,128)(4,1)S(1)} %broadcast_in_dim.115, pred[6,1024]{1,0:T(8,128)(4,1)S(1)} %broadcast_in_dim.107, pred[6,1024]{1,0:T(8,128)(4,1)S(1)} %broadcast_in_dim.104, bf16[6,1024,1024]{2,1,0:T(8,128)(2,1)} %bitcast.81, bf16[6,1024,1024]{2,1,0:T(8,128)(2,1)} %bitcast.82), kind=kLoop, calls=%fused_computation.6 | loop fusion | flops 18874368 | bytes 37767168 | tf_op jit(solution)/shard_map/jit(_where)/select_n | solution.py:74
  156.0 5.2 %fusion.27 = (bf16[6,1024,512]{2,1,0:T(8,128)(2,1)}, bf16[6,1024,512]{2,1,0:T(8,128)(2,1)}) fusion(bf16[6,1024,1024]{2,1,0:T(8,128)(2,1)S(1)} %fusion), kind=kLoop, calls=%fused_computation.97 | loop fusion | bytes 25165824 | tf_op jit(solution)/shard_map/slice | solution.py:76
  161.2 8.6 %copy.88 = bf16[6,1024,512]{1,2,0:T(8,128)(2,1)} copy(bf16[6,1024,512]{2,1,0:T(8,128)(2,1)} %get-tuple-element.9) | data formatting | bytes 12582912 | tf_op jit(solution)/shard_map/slice | solution.py:76
  169.8 8.7 %copy.87 = bf16[6,1024,512]{1,2,0:T(8,128)(2,1)} copy(bf16[6,1024,512]{2,1,0:T(8,128)(2,1)} %get-tuple-element.10) | data formatting | bytes 12582912 | tf_op jit(solution)/shard_map/slice | solution.py:77
  178.5 9.8 %fusion.3 = (f32[6,4,2,64]{3,2,1,0:T(2,128)S(1)}, f32[6,4,1024,64,2]{2,3,4,1,0:T(8,128)}) fusion(pred[6,64,1024]{2,1,0:T(8,128)(4,1)S(1)} %compare_and_fusion, bf16[6,1024,4,128,1]{1,3,4,2,0:T(8,128)(2,1)} %bitcast.83, bf16[6,64,4,2,128]{4,3,2,1,0:T(2,128)(2,1)S(1)} %reshape.489), kind=kOutput, calls=%fused_computation.11 | convolution fusion | flops 814740480 | bytes 20066304 | tf_op jit(solution)/shard_map/bqkgd,bskd->bkgqs/dot_general | solution.py:79
  188.3 6.6 %fusion.1 = f32[6,4,2,64]{3,2,1,0:T(2,128)S(1)} fusion(f32[6,4,1024,64,2]{2,3,4,1,0:T(8,128)} %get-tuple-element.35, f32[6,4,2,64]{3,2,1,0:T(2,128)S(1)} %get-tuple-element.34, pred[6,64,1024]{2,1,0:T(8,128)(4,1)S(1)} %compare_and_fusion), kind=kLoop, calls=%fused_computation.9 | loop fusion | flops 12579840 | bytes 13000704 | tf_op jit(solution)/shard_map/reduce_sum | solution.py:100
  194.9 9.9 %fusion.10 = bf16[6,64,4,2,128]{4,1,3,2,0:T(8,128)(2,1)S(1)} fusion(bf16[6,1024,4,128,1]{1,3,4,2,0:T(8,128)(2,1)} %bitcast.85, f32[6,4,1024,64,2]{2,3,4,1,0:T(8,128)} %get-tuple-element.35, f32[6,4,2,64]{3,2,1,0:T(2,128)S(1)} %get-tuple-element.34, pred[6,64,1024]{2,1,0:T(8,128)(4,1)S(1)} %compare_and_fusion, f32[6,64,4,2]{1,3,2,0:T(2,128)S(1)} %bitcast.86), kind=kOutput, calls=%fused_computation.19 | convolution fusion | flops 818675712 | bytes 20078592 | tf_op jit(solution)/shard_map/bkgqs,bskd->bqkgd/dot_general | solution.py:101
  207.1 23.4 %all-gather.5.cloned.1.call-done = bf16[384,2048]{1,0:T(8,128)(2,1)} async-done(((bf16[384,1024]{1,0:T(8,128)(2,1)}), bf16[384,2048]{1,0:T(8,128)(2,1)}) %all-gather.5.cloned.1.call-update) | async-done | bytes 1572880 | tf_op jit(solution)/shard_map/all_gather | solution.py:110
  230.4 5.3 %convolution_convert_fusion = bf16[384,1024]{1,0:T(8,128)(2,1)} fusion(bf16[384,2048]{1,0:T(8,128)(2,1)} %all-gather.5.cloned.1.call-done, bf16[2048,1024]{1,0:T(8,128)(2,1)} %param.10), kind=kOutput, calls=%fused_computation.21 | convolution fusion | flops 1611005952 | bytes 6553600 | tf_op jit(solution)/shard_map/dot_general | solution.py:109
  (87 shorter events, 20.6 us)
Async XLA Ops:
  6.5 38.9 %copy-start = (bf16[2048,512]{1,0:T(8,128)(2,1)S(1)}, bf16[2048,512]{1,0:T(8,128)(2,1)}, u32[]{:S(2)}) copy-start(bf16[2048,512]{1,0:T(8,128)(2,1)} %param.9) | copy-start | bytes 6291460
  6.5 38.9 %all-gather.3.cloned.1.call-start = ((), (), s32[]{:S(2)}) async-start(), calls=%async_computation.1 | async-start | bytes 2359296 | tf_op jit(solution)/shard_map/all_gather | solution.py:33
  9.6 9.8 %collective-permute-start.14 = (s32[1,2]{0,1:T(2,128)S(1)}, s32[1,2]{0,1:T(2,128)S(1)}, u32[]{:S(2)}, u32[]{:S(2)}) collective-permute-start(s32[1,2]{0,1:T(2,128)S(1)} %get-tuple-element.16), channel_id=1, source_target_pairs={{0,30},{2,0},{4,2},{6,4},{8,6},{10,8},{12,10},{14,12},{16,14},{18,... | collective-permute-start | bytes 32 | tf_op jit(solution)/shard_map/ppermute | solution.py:64
  16.6 7.3 %collective-permute-start.13 = (s32[1,2]{0,1:T(2,128)S(1)}, s32[1,2]{0,1:T(2,128)S(1)}, u32[]{:S(2)}, u32[]{:S(2)}) collective-permute-start(s32[1,2]{0,1:T(2,128)S(1)} %get-tuple-element.17), channel_id=1, source_target_pairs={{0,28},{2,30},{4,0},{6,2},{8,4},{10,6},{12,8},{14,10},{16,12},{18,... | collective-permute-start | bytes 32 | tf_op jit(solution)/shard_map/ppermute | solution.py:64
  17.1 6.8 %collective-permute-start.12 = (s32[1,2]{0,1:T(2,128)S(1)}, s32[1,2]{0,1:T(2,128)S(1)}, u32[]{:S(2)}, u32[]{:S(2)}) collective-permute-start(s32[1,2]{0,1:T(2,128)S(1)} %get-tuple-element.18), channel_id=1, source_target_pairs={{0,26},{2,28},{4,30},{6,0},{8,2},{10,4},{12,6},{14,8},{16,10},{18,... | collective-permute-start | bytes 32 | tf_op jit(solution)/shard_map/ppermute | solution.py:64
  17.6 7.9 %collective-permute-start.11 = (s32[1,2]{0,1:T(2,128)S(1)}, s32[1,2]{0,1:T(2,128)S(1)}, u32[]{:S(2)}, u32[]{:S(2)}) collective-permute-start(s32[1,2]{0,1:T(2,128)S(1)} %get-tuple-element.19), channel_id=1, source_target_pairs={{0,24},{2,26},{4,28},{6,30},{8,0},{10,2},{12,4},{14,6},{16,8},{18,... | collective-permute-start | bytes 32 | tf_op jit(solution)/shard_map/ppermute | solution.py:64
  18.1 10.0 %collective-permute-start.10 = (s32[1,2]{0,1:T(2,128)S(1)}, s32[1,2]{0,1:T(2,128)S(1)}, u32[]{:S(2)}, u32[]{:S(2)}) collective-permute-start(s32[1,2]{0,1:T(2,128)S(1)} %get-tuple-element.20), channel_id=1, source_target_pairs={{0,22},{2,24},{4,26},{6,28},{8,30},{10,0},{12,2},{14,4},{16,6},{18... | collective-permute-start | bytes 32 | tf_op jit(solution)/shard_map/ppermute | solution.py:64
  19.4 11.2 %collective-permute-start.9 = (s32[1,2]{0,1:T(2,128)S(1)}, s32[1,2]{0,1:T(2,128)S(1)}, u32[]{:S(2)}, u32[]{:S(2)}) collective-permute-start(s32[1,2]{0,1:T(2,128)S(1)} %get-tuple-element.21), channel_id=1, source_target_pairs={{0,20},{2,22},{4,24},{6,26},{8,28},{10,30},{12,0},{14,2},{16,4},{1... | collective-permute-start | bytes 32 | tf_op jit(solution)/shard_map/ppermute | solution.py:64
  23.9 7.4 %collective-permute-start.8 = (s32[1,2]{0,1:T(2,128)S(1)}, s32[1,2]{0,1:T(2,128)S(1)}, u32[]{:S(2)}, u32[]{:S(2)}) collective-permute-start(s32[1,2]{0,1:T(2,128)S(1)} %get-tuple-element.22), channel_id=1, source_target_pairs={{0,18},{2,20},{4,22},{6,24},{8,26},{10,28},{12,30},{14,0},{16,2},{... | collective-permute-start | bytes 32 | tf_op jit(solution)/shard_map/ppermute | solution.py:64
  23.9 9.2 %collective-permute-start.7 = (s32[1,2]{0,1:T(2,128)S(1)}, s32[1,2]{0,1:T(2,128)S(1)}, u32[]{:S(2)}, u32[]{:S(2)}) collective-permute-start(s32[1,2]{0,1:T(2,128)S(1)} %get-tuple-element.23), channel_id=1, source_target_pairs={{0,16},{2,18},{4,20},{6,22},{8,24},{10,26},{12,28},{14,30},{16,0},... | collective-permute-start | bytes 32 | tf_op jit(solution)/shard_map/ppermute | solution.py:64
  25.5 10.9 %collective-permute-start.6 = (s32[1,2]{0,1:T(2,128)S(1)}, s32[1,2]{0,1:T(2,128)S(1)}, u32[]{:S(2)}, u32[]{:S(2)}) collective-permute-start(s32[1,2]{0,1:T(2,128)S(1)} %get-tuple-element.24), channel_id=1, source_target_pairs={{0,14},{2,16},{4,18},{6,20},{8,22},{10,24},{12,26},{14,28},{16,30}... | collective-permute-start | bytes 32 | tf_op jit(solution)/shard_map/ppermute | solution.py:64
  28.1 9.2 %collective-permute-start.5 = (s32[1,2]{0,1:T(2,128)S(1)}, s32[1,2]{0,1:T(2,128)S(1)}, u32[]{:S(2)}, u32[]{:S(2)}) collective-permute-start(s32[1,2]{0,1:T(2,128)S(1)} %get-tuple-element.25), channel_id=1, source_target_pairs={{0,12},{2,14},{4,16},{6,18},{8,20},{10,22},{12,24},{14,26},{16,28}... | collective-permute-start | bytes 32 | tf_op jit(solution)/shard_map/ppermute | solution.py:64
  30.6 6.7 %collective-permute-start.4 = (s32[1,2]{0,1:T(2,128)S(1)}, s32[1,2]{0,1:T(2,128)S(1)}, u32[]{:S(2)}, u32[]{:S(2)}) collective-permute-start(s32[1,2]{0,1:T(2,128)S(1)} %get-tuple-element.26), channel_id=1, source_target_pairs={{0,10},{2,12},{4,14},{6,16},{8,18},{10,20},{12,22},{14,24},{16,26}... | collective-permute-start | bytes 32 | tf_op jit(solution)/shard_map/ppermute | solution.py:64
  31.3 6.0 %collective-permute-start.3 = (s32[1,2]{0,1:T(2,128)S(1)}, s32[1,2]{0,1:T(2,128)S(1)}, u32[]{:S(2)}, u32[]{:S(2)}) collective-permute-start(s32[1,2]{0,1:T(2,128)S(1)} %get-tuple-element.27), channel_id=1, source_target_pairs={{0,8},{2,10},{4,12},{6,14},{8,16},{10,18},{12,20},{14,22},{16,24},... | collective-permute-start | bytes 32 | tf_op jit(solution)/shard_map/ppermute | solution.py:64
  33.2 7.2 %collective-permute-start.2 = (s32[1,2]{0,1:T(2,128)S(1)}, s32[1,2]{0,1:T(2,128)S(1)}, u32[]{:S(2)}, u32[]{:S(2)}) collective-permute-start(s32[1,2]{0,1:T(2,128)S(1)} %get-tuple-element.28), channel_id=1, source_target_pairs={{0,6},{2,8},{4,10},{6,12},{8,14},{10,16},{12,18},{14,20},{16,22},{... | collective-permute-start | bytes 32 | tf_op jit(solution)/shard_map/ppermute | solution.py:64
  36.4 6.3 %collective-permute-start.1 = (s32[1,2]{0,1:T(2,128)S(1)}, s32[1,2]{0,1:T(2,128)S(1)}, u32[]{:S(2)}, u32[]{:S(2)}) collective-permute-start(s32[1,2]{0,1:T(2,128)S(1)} %get-tuple-element.29), channel_id=1, source_target_pairs={{0,4},{2,6},{4,8},{6,10},{8,12},{10,14},{12,16},{14,18},{16,20},{1... | collective-permute-start | bytes 32 | tf_op jit(solution)/shard_map/ppermute | solution.py:64
  37.3 7.2 %collective-permute-start = (s32[1,2]{0,1:T(2,128)S(1)}, s32[1,2]{0,1:T(2,128)S(1)}, u32[]{:S(2)}, u32[]{:S(2)}) collective-permute-start(s32[1,2]{0,1:T(2,128)S(1)} %get-tuple-element.30), channel_id=1, source_target_pairs={{0,2},{2,4},{4,6},{6,8},{8,10},{10,12},{12,14},{14,16},{16,18},{18... | collective-permute-start | bytes 32 | tf_op jit(solution)/shard_map/ppermute | solution.py:64
  58.3 5.0 %copy-start.2 = (s32[6,16]{1,0:T(8,128)S(1)}, s32[6,16]{1,0:T(8,128)}, u32[]{:S(2)}) copy-start(s32[6,16]{1,0:T(8,128)} %param.11) | copy-start | bytes 1156
  58.3 80.1 %all-to-all-start = ((bf16[16,2,64,1024]{3,2,1,0:T(8,128)(2,1)}), bf16[16,2,64,1024]{3,2,1,0:T(8,128)(2,1)}, u32[]{:S(2)}, u32[]{:S(2)}) async-start(bf16[16,2,64,1024]{3,2,1,0:T(8,128)(2,1)} %broadcast_select_fusion), calls=%async_computation | async-start | bytes 8388608 | tf_op jit(solution)/shard_map/all_to_all | solution.py:70
  63.0 167.4 %all-gather.5.cloned.1.call-start = ((), (), s32[]{:S(2)}) async-start(), calls=%async_computation.2 | async-start | bytes 2359296 | tf_op jit(solution)/shard_map/all_gather | solution.py:110
  205.6 30.2 %copy-start.1 = (bf16[2048,512]{1,0:T(8,128)(2,1)S(1)}, bf16[2048,512]{1,0:T(8,128)(2,1)}, u32[]{:S(2)}) copy-start(bf16[2048,512]{1,0:T(8,128)(2,1)} %param.9) | copy-start | bytes 6291460
Sparse Core Ops, SparseCore 0:
  8.9 12.5 all-gather.2
  207.2 23.1 all-gather.4
